TPU v7x, 32 devices: a whole 2x2x4 slice. The times are simulated.
32 devices in a mesh: grp: 2 (over x), sp: 4 (over z), tp: 4 (over y, core).
Axes of the slice: x: 2, y: 2, z: 4, core: 2. Of those that a mesh axis runs over, the one named last changes fastest.
Arguments:
- tokens: bfloat16 [1792, 4096], P(('grp', 'sp'), 'tp'), parts along dimension 0, may hold values from -130 to 130
- rms_gain: float32 [2, 4096], replicated, may hold values from 0.1 to 1.9
- w_value: bfloat16 [2, 4096, 2048], P(None, 'sp', 'tp'), may hold values from -0.09375 to 0.09375
- w_gate: bfloat16 [2, 4096, 2048], P(None, 'sp', 'tp'), may hold values from -0.09375 to 0.09375
- taps: float32 [2, 31, 2048], P(None, None, 'tp'), may hold values from -8 to 8
- ln_gain: float32 [2, 2048], P(None, 'tp'), may hold values from 0.1 to 1.9
- ln_bias: float32 [2, 2048], P(None, 'tp'), may hold values from -3 to 3
- w_out: bfloat16 [2, 2048, 4096], P(None, 'sp', 'tp'), may hold values from -0.125 to 0.125
Outputs:
- result: bfloat16 [1792, 4096], P(('grp', 'sp'), 'tp'), parts along dimension 0
There are 2 independent parts, one for each index of `grp`. A program takes and returns all parts, laid end to end along the dimension named above; an argument that names none is the same for every part. Nothing has to cross between parts.
All inputs are finite; a program needn't handle non-finite values.
Results may differ from a plain program's by a relative error of at most 0.009.
Values may be sent and summed in bfloat16 or wider, within the bound.
A program may use at most 64 MiB of HBM per device.

v0:
```python
import jax
import jax.numpy as jnp
from jax import lax
from jax.sharding import PartitionSpec as P

CH = 2048


def passed_along(block, axis, distance):
    devices = range(lax.axis_size(axis))
    route = [(i - distance, i) for i in devices if i - distance in devices]
    return lax.ppermute(block, axis, route)


def project_in(weight, columns):
    return lax.dot_general(
        weight, columns, (((0,), (1,)), ((), ())), preferred_element_type=jnp.float32
    )


def project_out(rows, weight):
    return lax.dot_general(
        rows, weight, (((0,), (0,)), ((), ())), preferred_element_type=jnp.float32
    )


def norm_rows(wide, gain):
    return (wide * lax.rsqrt(jnp.mean(wide * wide, axis=1, keepdims=True) + 1e-06) * gain).astype(
        jnp.bfloat16
    )


def shards(tokens, rms_gain, w_value, w_gate, taps, ln_gain, ln_bias, w_out):
    layers = w_value.shape[0]
    tok_rows = tokens.shape[0]
    chans = w_value.shape[2]
    reach = taps.shape[1]
    current = tokens
    for layer in range(layers):
        gain = rms_gain[layer]
        whole_rows = lax.all_gather(current, "tp", axis=1, tiled=True)
        normed = norm_rows(whole_rows.astype(jnp.float32), gain)
        value_t = project_in(lax.all_gather(w_value[layer], "sp", axis=0, tiled=True), normed)
        gate_t = project_in(lax.all_gather(w_gate[layer], "sp", axis=0, tiled=True), normed)
        glu_t = (value_t * jax.nn.sigmoid(gate_t)).astype(jnp.bfloat16)
        earlier = passed_along(glu_t[:, tok_rows - (reach - 1) :], "sp", 1)
        extended = jnp.concatenate([earlier, glu_t], axis=1).astype(jnp.float32)
        layer_taps = taps[layer]
        conv = jnp.zeros((chans, tok_rows), jnp.float32)
        for k in range(reach):
            conv = conv + layer_taps[k][:, None] * extended[:, k : k + tok_rows]
        total, total_sq = lax.psum((jnp.sum(conv, axis=0), jnp.sum(conv * conv, axis=0)), "tp")
        mean = total / CH
        var = total_sq / CH - mean * mean
        shaped = (conv - mean[None, :]) * lax.rsqrt(var + 1e-05)[None, :] * ln_gain[layer][
            :, None
        ] + ln_bias[layer][:, None]
        act_t = jax.nn.silu(shaped).astype(jnp.bfloat16)
        act_all = lax.all_gather(act_t, "tp", axis=0, tiled=True)
        branch = project_out(act_all, lax.all_gather(w_out[layer], "sp", axis=0, tiled=True))
        current = (current.astype(jnp.float32) + branch).astype(jnp.bfloat16)
    return current


def solution(mesh):
    return jax.shard_map(
        shards,
        mesh=mesh,
        in_specs=(
            P(("grp", "sp"), "tp"),
            P(),
            P(None, "sp", "tp"),
            P(None, "sp", "tp"),
            P(None, None, "tp"),
            P(None, "tp"),
            P(None, "tp"),
            P(None, "sp", "tp"),
        ),
        out_specs=P(("grp", "sp"), "tp"),
        check_vma=False,
    )
```

profile of v0, /device:TPU:21, one launch (start us, length us, event | category | flops | bytes accessed | tf_op | source)
XLA Modules:
  0.0 551.9 jit_solution(11916564640636365866)
XLA Ops:
  6.5 0.7 all-gather.15.cloned.1.call-update
  7.3 0.0 all-gather.21.cloned.1.call-start
  7.3 3.0 fusion.142
  10.3 0.0 all-gather.21.cloned.1.call-update
  10.3 0.0 all-gather.19.cloned.1.call-start
  10.4 1.5 fusion.141
  11.9 0.0 all-gather.19.cloned.1.call-update
  11.9 0.0 all-gather.23.cloned.1.call-start
  11.9 3.0 fusion.140
  15.0 0.0 all-gather.23.cloned.1.call-update
  15.0 0.0 all-gather.17.cloned.1.call-start
  15.2 15.3 %all-gather.15.cloned.1.call-done = bf16[224,4096]{1,0:T(8,128)(2,1)} async-done(((bf16[224,1024]{1,0:T(8,128)(2,1)}), bf16[224,4096]{1,0:T(8,128)(2,1)}) %all-gather.15.cloned.1.call-update) | async-done | bytes 1835024 | tf_op jit(solution)/shard_map/all_gather | solution.py:41
  30.5 1.9 fusion.12
  32.5 79.2 %all-gather.21.cloned.1.call-done = bf16[1,4096,512]{2,1,0:T(8,128)(2,1)} async-done(((bf16[1,1024,512]{2,1,0:T(8,128)(2,1)}), bf16[1,4096,512]{2,1,0:T(8,128)(2,1)}) %all-gather.21.cloned.1.call-update) | async-done | bytes 4194320 | tf_op jit(solution)/shard_map/all_gather | solution.py:44
  111.7 4.1 fusion.57
  115.9 76.7 %all-gather.19.cloned.1.call-done = bf16[1,4096,512]{2,1,0:T(8,128)(2,1)} async-done(((bf16[1,1024,512]{2,1,0:T(8,128)(2,1)}), bf16[1,4096,512]{2,1,0:T(8,128)(2,1)}) %all-gather.19.cloned.1.call-update) | async-done | bytes 4194320 | tf_op jit(solution)/shard_map/all_gather | solution.py:43
  192.6 3.3 fusion.66
  195.9 2.4 collective-permute-start
  198.4 2.2 collective-permute-done
  200.6 0.1 maximum_convert_fusion
  200.7 2.4 fusion.137
  203.0 7.0 %all-reduce.1 = (f32[224]{0:T(256)S(1)}, f32[224]{0:T(256)S(1)}) all-reduce(f32[224]{0:T(256)S(1)} %get-tuple-element.8, f32[224]{0:T(256)S(1)} %get-tuple-element.7), channel_id=1, replica_groups=mesh['grp'=2,'sp'=4,'tp'=4] {'tp'}, use_global_device_ids=true, to_apply=%region_4.0 | all-reduce | flops 448 | bytes 3584 | tf_op jit(solution)/shard_map/psum | solution.py:52
  210.1 0.2 multiply_convert_fusion.1
  210.3 9.4 %all_gather.33 = bf16[2048,224]{0,1:T(8,128)(2,1)S(1)} all-gather(bf16[512,224]{0,1:T(8,128)(2,1)S(1)} %multiply_convert_fusion.1), channel_id=1, replica_groups=mesh['grp'=2,'sp'=4,'tp'=4] {'tp'}, dimensions={0}, use_global_device_ids=true | all-gather | bytes 1146880 | tf_op jit(solution)/shard_map/all_gather | solution.py:59
  219.7 53.5 %all-gather.23.cloned.1.call-done = bf16[1,2048,1024]{2,1,0:T(8,128)(2,1)} async-done(((bf16[1,512,1024]{2,1,0:T(8,128)(2,1)}), bf16[1,2048,1024]{2,1,0:T(8,128)(2,1)}) %all-gather.23.cloned.1.call-update) | async-done | bytes 4194320 | tf_op jit(solution)/shard_map/all_gather | solution.py:60
  273.2 4.1 fusion.27
  277.3 0.0 all-gather.17.cloned.1.call-update
  277.4 0.0 all-gather.27.cloned.1.call-start
  277.4 0.5 all-gather.27.cloned.1.call-update
  277.9 0.0 all-gather.25.cloned.1.call-start
  278.0 0.7 all-gather.25.cloned.1.call-update
  278.7 0.0 all-gather.29.cloned.1.call-start
  278.7 0.7 all-gather.29.cloned.1.call-update
  279.4 18.8 %all-gather.17.cloned.1.call-done = bf16[224,4096]{1,0:T(8,128)(2,1)} async-done(((bf16[224,1024]{1,0:T(8,128)(2,1)}), bf16[224,4096]{1,0:T(8,128)(2,1)}) %all-gather.17.cloned.1.call-update) | async-done | bytes 1835024 | tf_op jit(solution)/shard_map/all_gather | solution.py:41
  298.2 1.9 fusion.15
  300.2 79.1 %all-gather.27.cloned.1.call-done = bf16[1,4096,512]{2,1,0:T(8,128)(2,1)} async-done(((bf16[1,1024,512]{2,1,0:T(8,128)(2,1)}), bf16[1,4096,512]{2,1,0:T(8,128)(2,1)}) %all-gather.27.cloned.1.call-update) | async-done | bytes 4194320 | tf_op jit(solution)/shard_map/all_gather | solution.py:44
  379.3 4.1 fusion.51
  383.4 76.7 %all-gather.25.cloned.1.call-done = bf16[1,4096,512]{2,1,0:T(8,128)(2,1)} async-done(((bf16[1,1024,512]{2,1,0:T(8,128)(2,1)}), bf16[1,4096,512]{2,1,0:T(8,128)(2,1)}) %all-gather.25.cloned.1.call-update) | async-done | bytes 4194320 | tf_op jit(solution)/shard_map/all_gather | solution.py:43
  460.1 3.3 fusion.69
  463.5 2.4 collective-permute-start.1
  466.0 2.2 collective-permute-done.1
  468.2 0.1 maximum_convert_fusion.1
  468.2 2.4 fusion.136
  470.6 7.0 %all-reduce = (f32[224]{0:T(256)S(1)}, f32[224]{0:T(256)S(1)}) all-reduce(f32[224]{0:T(256)S(1)} %get-tuple-element.6, f32[224]{0:T(256)S(1)} %get-tuple-element.5), channel_id=1, replica_groups=mesh['grp'=2,'sp'=4,'tp'=4] {'tp'}, use_global_device_ids=true, to_apply=%region_9.10 | all-reduce | flops 448 | bytes 3584 | tf_op jit(solution)/shard_map/psum | solution.py:52
  477.7 0.2 multiply_convert_fusion
  477.9 9.4 %all_gather.38 = bf16[2048,224]{0,1:T(8,128)(2,1)S(1)} all-gather(bf16[512,224]{0,1:T(8,128)(2,1)S(1)} %multiply_convert_fusion), channel_id=1, replica_groups=mesh['grp'=2,'sp'=4,'tp'=4] {'tp'}, dimensions={0}, use_global_device_ids=true | all-gather | bytes 1146880 | tf_op jit(solution)/shard_map/all_gather | solution.py:59
  487.3 53.6 %all-gather.29.cloned.1.call-done = bf16[1,2048,1024]{2,1,0:T(8,128)(2,1)} async-done(((bf16[1,512,1024]{2,1,0:T(8,128)(2,1)}), bf16[1,2048,1024]{2,1,0:T(8,128)(2,1)}) %all-gather.29.cloned.1.call-update) | async-done | bytes 4194320 | tf_op jit(solution)/shard_map/all_gather | solution.py:60
  541.0 4.1 fusion.24
  (32 shorter events, 0.3 us)
Async XLA Ops:
  6.5 3.9 copy-start
  6.5 24.0 %all-gather.15.cloned.1.call-start = ((), (), s32[]{:S(2)}) async-start(), calls=%async_computation | async-start | bytes 2293760 | tf_op jit(solution)/shard_map/all_gather | solution.py:41
  7.3 104.5 %all-gather.21.cloned.1.call-start = ((), (), s32[]{:S(2)}) async-start(), calls=%async_computation.3 | async-start | bytes 5242880 | tf_op jit(solution)/shard_map/all_gather | solution.py:44
  10.3 182.2 %all-gather.19.cloned.1.call-start = ((), (), s32[]{:S(2)}) async-start(), calls=%async_computation.2 | async-start | bytes 5242880 | tf_op jit(solution)/shard_map/all_gather | solution.py:43
  11.9 3.2 copy-start.7
  11.9 3.2 copy-start.5
  11.9 3.3 copy-start.6
  11.9 261.4 %all-gather.23.cloned.1.call-start = ((), (), s32[]{:S(2)}) async-start(), calls=%async_computation.4 | async-start | bytes 5242880 | tf_op jit(solution)/shard_map/all_gather | solution.py:60
  15.0 283.2 %all-gather.17.cloned.1.call-start = ((), (), s32[]{:S(2)}) async-start(), calls=%async_computation.1 | async-start | bytes 2293760 | tf_op jit(solution)/shard_map/all_gather | solution.py:41
  111.7 80.8 %copy-start.1 = (bf16[224,4096]{1,0:T(8,128)(2,1)S(1)}, bf16[224,4096]{1,0:T(8,128)(2,1)}, u32[]{:S(2)}) copy-start(bf16[224,4096]{1,0:T(8,128)(2,1)} %all-gather.15.cloned.1.call-done) | copy-start | bytes 5505028
  115.8 82.5 %copy-start.8 = (f32[2,512]{1,0:T(2,128)S(1)}, f32[2,512]{1,0:T(2,128)}, u32[]{:S(2)}) copy-start(f32[2,512]{1,0:T(2,128)} %param.14) | copy-start | bytes 12292
  195.9 4.7 collective-permute-start
  200.7 72.6 %copy-start.3 = (bf16[224,1024]{1,0:T(8,128)(2,1)S(1)}, bf16[224,1024]{1,0:T(8,128)(2,1)}, u32[]{:S(2)}) copy-start(bf16[224,1024]{1,0:T(8,128)(2,1)} %param.8) | copy-start | bytes 1376260
  277.4 101.9 %all-gather.27.cloned.1.call-start = ((), (), s32[]{:S(2)}) async-start(), calls=%async_computation.6 | async-start | bytes 5242880 | tf_op jit(solution)/shard_map/all_gather | solution.py:44
  277.9 182.2 %all-gather.25.cloned.1.call-start = ((), (), s32[]{:S(2)}) async-start(), calls=%async_computation.5 | async-start | bytes 5242880 | tf_op jit(solution)/shard_map/all_gather | solution.py:43
  278.7 262.3 %all-gather.29.cloned.1.call-start = ((), (), s32[]{:S(2)}) async-start(), calls=%async_computation.7 | async-start | bytes 5242880 | tf_op jit(solution)/shard_map/all_gather | solution.py:60
  379.3 80.8 %copy-start.2 = (bf16[224,4096]{1,0:T(8,128)(2,1)S(1)}, bf16[224,4096]{1,0:T(8,128)(2,1)}, u32[]{:S(2)}) copy-start(bf16[224,4096]{1,0:T(8,128)(2,1)} %all-gather.17.cloned.1.call-done) | copy-start | bytes 5505028
  463.5 4.7 collective-permute-start.1
  468.2 72.7 %copy-start.4 = (bf16[224,1024]{1,0:T(8,128)(2,1)S(1)}, bf16[224,1024]{1,0:T(8,128)(2,1)}, u32[]{:S(2)}) copy-start(bf16[224,1024]{1,0:T(8,128)(2,1)} %fusion.27) | copy-start | bytes 1376260
Sparse Core Ops, SparseCore 0:
  8.9 21.5 all-gather.14
  32.1 79.5 all-gather.20
  113.3 79.2 all-gather.18
  194.0 79.2 all-gather.22
  277.5 20.7 all-gather.16
  299.7 79.5 all-gather.26
  380.9 79.2 all-gather.24
  461.7 79.2 all-gather.28
where the time goes:
time: 556 us; the launch traced here: 552 us
  waiting for transfers between devices  460 us (83%)
  blocking collectives  32.9 us (6%)
  matrix products  23.1 us (4%)
  between operations  13.7 us (2%)
  other arithmetic  9.31 us (2%)
  local copies, waits for them, and re-layouts  7.75 us (1%)
    all_gather x2, waiting for transfers between devices, shards(): lax.all_gather(w_gate[layer], 'sp', axis=0, tiled=True)  158 us
    all_gather x2, waiting for transfers between devices, shards(): lax.all_gather(w_value[layer], 'sp', axis=0, tiled=True)  153 us
    all_gather x2, waiting for transfers between devices, shards(): lax.all_gather(w_out[layer], 'sp', axis=0, tiled=True)  107 us
    all_gather x2, waiting for transfers between devices, shards(): whole_rows = lax.all_gather(current, 'tp', axis=1, tiled=True)  34.1 us
    all_gather x2, blocking collectives, shards(): act_all = lax.all_gather(act_t, 'tp', axis=0, tiled=True)  18.8 us
    dot_general x4, matrix products, project_in(): lax.dot_general(weight, columns, (((0,), (1,)), ((), ())), preferred_elem...  14.9 us
    psum x2, blocking collectives, shards(): lax.psum((jnp.sum(conv, axis=0), jnp.sum(conv * conv, axis=0)), 'tp')  14 us
  transfers between devices with their start and end apart: 10, of which 10 were waited for; matrix products, arithmetic and copies ran while one was open for 6% of the time, Pallas kernels for 0%

commit v1 on v0

v1 whole, which is shorter than its diff:
```python
import jax
import jax.numpy as jnp
from jax import lax
from jax.sharding import PartitionSpec as P


def passed_along(block, axis, distance):
    devices = range(lax.axis_size(axis))
    route = [(i - distance, i) for i in devices if i - distance in devices]
    return lax.ppermute(block, axis, route)


def norm_rows(wide, gain):
    return (wide * lax.rsqrt(jnp.mean(wide * wide, axis=1, keepdims=True) + 1e-06) * gain).astype(
        jnp.bfloat16
    )


def to_depth(rows):
    return lax.all_to_all(rows, "sp", split_axis=1, concat_axis=0, tiled=True)


def summed(partial):
    sp = lax.axis_size("sp")
    rows = partial.shape[0] // sp
    parts = partial.astype(jnp.bfloat16).reshape(sp, rows, partial.shape[1])
    parts = lax.all_to_all(parts, "sp", split_axis=0, concat_axis=0, tiled=True)
    return jnp.sum(parts.astype(jnp.float32), axis=0)


def shards(tokens, rms_gain, w_value, w_gate, taps, ln_gain, ln_bias, w_out):
    layers = w_value.shape[0]
    tok_rows = tokens.shape[0]
    chans = w_value.shape[2]
    all_chans = chans * lax.axis_size("tp")
    reach = taps.shape[1]
    current = tokens
    for layer in range(layers):
        whole_rows = lax.all_gather(current, "tp", axis=1, tiled=True)
        normed = to_depth(norm_rows(whole_rows.astype(jnp.float32), rms_gain[layer]))
        both = jnp.concatenate([w_value[layer], w_gate[layer]], axis=1)
        both = summed(jnp.dot(normed, both, preferred_element_type=jnp.float32))
        glu = (both[:, :chans] * jax.nn.sigmoid(both[:, chans:])).astype(jnp.bfloat16)
        earlier = passed_along(glu[tok_rows - (reach - 1) :], "sp", 1)
        extended = jnp.concatenate([earlier, glu], axis=0).astype(jnp.float32)
        conv = jnp.zeros((tok_rows, chans), jnp.float32)
        for k in range(reach):
            conv = conv + taps[layer, k][None, :] * extended[k : k + tok_rows]
        total, total_sq = lax.psum((jnp.sum(conv, axis=1), jnp.sum(conv * conv, axis=1)), "tp")
        mean = total / all_chans
        var = total_sq / all_chans - mean * mean
        shaped = (conv - mean[:, None]) * lax.rsqrt(var + 1e-05)[:, None] * ln_gain[layer][
            None, :
        ] + ln_bias[layer][None, :]
        act = jax.nn.silu(shaped).astype(jnp.bfloat16)
        act_all = to_depth(lax.all_gather(act, "tp", axis=1, tiled=True))
        branch = summed(jnp.dot(act_all, w_out[layer], preferred_element_type=jnp.float32))
        current = (current.astype(jnp.float32) + branch).astype(jnp.bfloat16)
    return current


def solution(mesh):
    return jax.shard_map(
        shards,
        mesh=mesh,
        in_specs=(
            P(("grp", "sp"), "tp"),
            P(),
            P(None, "sp", "tp"),
            P(None, "sp", "tp"),
            P(None, None, "tp"),
            P(None, "tp"),
            P(None, "tp"),
            P(None, "sp", "tp"),
        ),
        out_specs=P(("grp", "sp"), "tp"),
        check_vma=False,
    )
```

time: 556 us -> 456 us (0.82)
  waiting for transfers between devices: 460 us -> 123 us
  blocking collectives: 32.9 us -> 264 us
  starting transfers between devices: 5.11 us -> 18.6 us
  matrix products: 23.1 us -> 9.66 us
    all_gather x6 -> x0, waiting for transfers between devices: 419 us -> none  [the longest x2 158 us: shards(): lax.all_gather(w_gate[layer], 'sp', axis=0, tiled=True)]
    all_to_all x0 -> x6, blocking collectives: none -> 228 us  [the longest x3 134 us: summed(): parts = lax.all_to_all(parts, 'sp', split_axis=0, concat_axis=0, tiled=True)]
    all_to_all x0 -> x2, waiting for transfers between devices: none -> 74.9 us  [the longest x1 39 us: summed(): parts = lax.all_to_all(parts, 'sp', split_axis=0, concat_axis=0, tiled=True)]
    dot_general x6 -> x4, matrix products: 23.1 us -> 9.66 us  [the longest x2 7.42 us: shards(): both = summed(jnp.dot(normed, both, preferred_element_type=jnp.float32))]
    all_to_all x0 -> x2, starting transfers between devices: none -> 11.5 us  [the longest x1 6.78 us: summed(): parts = lax.all_to_all(parts, 'sp', split_axis=0, concat_axis=0, tiled=True)]
    all_gather x2, waiting for transfers between devices: 34.1 us -> 45.2 us  [shards(): whole_rows = lax.all_gather(current, 'tp', axis=1, tiled=True)]
    slice x12 -> x9, local copies, waits for them, and re-layouts: 7.71 us -> 1.03 us  [the longest x1 0.86 us: shards(): rms_gain[layer]]
  transfers between devices with their start and end apart: 10 -> 6, of which waited for: 10 -> 6; matrix products, arithmetic and copies ran while one was open for 6% -> 1% of each run, Pallas kernels for 0% -> 0%
where the time goes in v1:
time: 456 us; the launch traced here: 450 us
  blocking collectives  264 us (58%)
  waiting for transfers between devices  123 us (27%)
  starting transfers between devices  18.6 us (4%)
  other arithmetic  14 us (3%)
  between operations  13.7 us (3%)
  matrix products  9.66 us (2%)
  local copies, waits for them, and re-layouts  7.39 us (2%)
    all_to_all x3, blocking collectives, summed(): parts = lax.all_to_all(parts, 'sp', split_axis=0, concat_axis=0, tiled=True)  134 us
    all_to_all x3, blocking collectives, to_depth(): return lax.all_to_all(rows, 'sp', split_axis=1, concat_axis=0, tiled=True)  94.4 us
    all_gather x2, waiting for transfers between devices, shards(): whole_rows = lax.all_gather(current, 'tp', axis=1, tiled=True)  45.2 us
    all_to_all x1, waiting for transfers between devices, summed(): parts = lax.all_to_all(parts, 'sp', split_axis=0, concat_axis=0, tiled=True)  39 us
    all_to_all x1, waiting for transfers between devices, to_depth(): return lax.all_to_all(rows, 'sp', split_axis=1, concat_axis=0, tiled=True)  35.9 us
    all_gather x2, blocking collectives, shards(): act_all = to_depth(lax.all_gather(act, 'tp', axis=1, tiled=True))  20.1 us
    psum x2, blocking collectives, shards(): lax.psum((jnp.sum(conv, axis=1), jnp.sum(conv * conv, axis=1)), 'tp')  15.1 us
  transfers between devices with their start and end apart: 6, of which 6 were waited for; matrix products, arithmetic and copies ran while one was open for 1% of the time, Pallas kernels for 0%

profile of v1, /device:TPU:21, one launch (start us, length us, event | category | flops | bytes accessed | tf_op | source)
XLA Modules:
  0.0 450.1 jit_solution(6833220004807300024)
XLA Ops:
  6.5 0.7 all-gather.3.cloned.1.call-update
  7.3 0.9 fusion.104
  8.1 22.4 %all-gather.3.cloned.1.call-done = bf16[224,4096]{1,0:T(8,128)(2,1)} async-done(((bf16[224,1024]{1,0:T(8,128)(2,1)}), bf16[224,4096]{1,0:T(8,128)(2,1)}) %all-gather.3.cloned.1.call-update) | async-done | bytes 1835024 | tf_op jit(solution)/shard_map/all_gather | solution.py:39
  30.5 2.1 fusion
  32.6 0.6 fusion.2
  33.2 1.4 copy.26
  34.5 4.7 %all-to-all-start = ((bf16[224,4,1024]{2,0,1:T(8,128)(2,1)}), bf16[224,4,1024]{2,0,1:T(8,128)(2,1)}, u32[]{:S(2)}, u32[]{:S(2)}) async-start(bf16[224,4,1024]{2,0,1:T(8,128)(2,1)} %bitcast.115), calls=%async_computation | async-start | bytes 3670016 | tf_op jit(solution)/shard_map/all_to_all | solution.py:20
  39.2 3.3 slice_bitcast_fusion
  42.5 35.9 %all-to-all-done = bf16[224,4,1024]{2,0,1:T(8,128)(2,1)} async-done(((bf16[224,4,1024]{2,0,1:T(8,128)(2,1)}), bf16[224,4,1024]{2,0,1:T(8,128)(2,1)}, u32[]{:S(2)}, u32[]{:S(2)}) %all-to-all-start) | async-done | bytes 1835040 | tf_op jit(solution)/shard_map/all_to_all | solution.py:20
  78.4 5.4 %fusion.17 = bf16[896,1024]{1,0:T(8,128)(2,1)} fusion(bf16[896,1024]{1,0:T(8,128)(2,1)} %bitcast.3, bf16[1024,512]{1,0:T(8,128)(2,1)} %get-tuple-element.18, bf16[1024,512]{1,0:T(8,128)(2,1)} %get-tuple-element.91), kind=kOutput, calls=%fused_computation.25 | convolution fusion | flops 1884160000 | bytes 5767168 | tf_op jit(solution)/shard_map/dot_general | solution.py:42
  83.8 6.8 %all-to-all-start.1 = ((bf16[4,224,1024]{2,1,0:T(8,128)(2,1)}), bf16[4,224,1024]{2,1,0:T(8,128)(2,1)S(1)}, u32[]{:S(2)}, u32[]{:S(2)}) async-start(bf16[4,224,1024]{2,1,0:T(8,128)(2,1)} %bitcast.125), calls=%async_computation.1 | async-start | bytes 3670016 | tf_op jit(solution)/shard_map/all_to_all | solution.py:27
  90.7 39.0 %all-to-all-done.1 = bf16[4,224,1024]{2,1,0:T(8,128)(2,1)S(1)} async-done(((bf16[4,224,1024]{2,1,0:T(8,128)(2,1)}), bf16[4,224,1024]{2,1,0:T(8,128)(2,1)S(1)}, u32[]{:S(2)}, u32[]{:S(2)}) %all-to-all-start.1) | async-done | bytes 1835040 | tf_op jit(solution)/shard_map/all_to_all | solution.py:27
  129.7 0.3 convert_reduce_fusion.3
  130.0 0.1 fusion.92
  130.2 3.1 collective-permute-start
  133.3 1.5 collective-permute-done
  134.9 2.4 fusion.97
  137.3 7.6 %all-reduce.1 = (f32[224]{0:T(256)S(1)}, f32[224]{0:T(256)S(1)}) all-reduce(f32[224]{0:T(256)S(1)} %get-tuple-element.8, f32[224]{0:T(256)S(1)} %get-tuple-element.7), channel_id=1, replica_groups=mesh['grp'=2,'sp'=4,'tp'=4] {'tp'}, use_global_device_ids=true, to_apply=%region_5.0 | all-reduce | flops 448 | bytes 3584 | tf_op jit(solution)/shard_map/psum | solution.py:49
  144.9 0.2 multiply_convert_fusion.1
  145.2 10.0 %all_gather.13 = bf16[224,2048]{1,0:T(8,128)(2,1)S(1)} all-gather(bf16[224,512]{1,0:T(8,128)(2,1)S(1)} %multiply_convert_fusion.1), channel_id=1, replica_groups=mesh['grp'=2,'sp'=4,'tp'=4] {'tp'}, dimensions={1}, use_global_device_ids=true | all-gather | bytes 1146880 | tf_op jit(solution)/shard_map/all_gather | solution.py:56
  155.2 0.1 copy.28
  155.3 25.4 %all_to_all.96 = bf16[224,4,512]{2,0,1:T(8,128)(2,1)S(1)} all-to-all(bf16[224,4,512]{2,0,1:T(8,128)(2,1)S(1)} %bitcast.121), channel_id=1, replica_groups=mesh['grp'=2,'sp'=4,'tp'=4] {'sp'}, dimensions={1} | all-to-all | bytes 1835008 | tf_op jit(solution)/shard_map/all_to_all | solution.py:20
  180.7 1.1 convolution_convert_fusion.1
  181.8 44.7 %all_to_all.97 = bf16[4,224,1024]{2,1,0:T(8,128)(2,1)S(1)} all-to-all(bf16[4,224,1024]{2,1,0:T(8,128)(2,1)S(1)} %bitcast.128), channel_id=1, replica_groups=mesh['grp'=2,'sp'=4,'tp'=4] {'sp'}, dimensions={0} | all-to-all | bytes 3670016 | tf_op jit(solution)/shard_map/all_to_all | solution.py:27
  226.5 0.3 convert_reduce_fusion.2
  226.8 0.7 copy-done.4
  227.5 0.9 add_convert_fusion.1
  228.4 22.8 %all-gather.5.cloned.1.call-done = bf16[224,4096]{1,0:T(8,128)(2,1)} async-done(((bf16[224,1024]{1,0:T(8,128)(2,1)}), bf16[224,4096]{1,0:T(8,128)(2,1)}) %all-gather.5.cloned.1.call-update) | async-done | bytes 1835024 | tf_op jit(solution)/shard_map/all_gather | solution.py:39
  251.2 2.1 fusion.3
  253.3 0.6 fusion.5
  253.9 0.2 copy.25
  254.1 44.2 %all_to_all.98 = bf16[224,4,1024]{2,0,1:T(8,128)(2,1)S(1)} all-to-all(bf16[224,4,1024]{2,0,1:T(8,128)(2,1)S(1)} %bitcast.118), channel_id=1, replica_groups=mesh['grp'=2,'sp'=4,'tp'=4] {'sp'}, dimensions={1} | all-to-all | bytes 3670016 | tf_op jit(solution)/shard_map/all_to_all | solution.py:20
  298.3 2.1 fusion.14
  300.3 44.7 %all_to_all.99 = bf16[4,224,1024]{2,1,0:T(8,128)(2,1)S(1)} all-to-all(bf16[4,224,1024]{2,1,0:T(8,128)(2,1)S(1)} %bitcast.127), channel_id=1, replica_groups=mesh['grp'=2,'sp'=4,'tp'=4] {'sp'}, dimensions={0} | all-to-all | bytes 3670016 | tf_op jit(solution)/shard_map/all_to_all | solution.py:27
  345.0 0.3 convert_reduce_fusion.1
  345.3 0.1 fusion.93
  345.5 4.0 collective-permute-start.1
  349.5 0.8 collective-permute-done.1
  350.4 2.4 fusion.96
  352.8 7.5 %all-reduce = (f32[224]{0:T(256)S(1)}, f32[224]{0:T(256)S(1)}) all-reduce(f32[224]{0:T(256)S(1)} %get-tuple-element.6, f32[224]{0:T(256)S(1)} %get-tuple-element.5), channel_id=1, replica_groups=mesh['grp'=2,'sp'=4,'tp'=4] {'tp'}, use_global_device_ids=true, to_apply=%region_12.13 | all-reduce | flops 448 | bytes 3584 | tf_op jit(solution)/shard_map/psum | solution.py:49
  360.3 0.2 multiply_convert_fusion
  360.5 10.0 %all_gather.15 = bf16[224,2048]{1,0:T(8,128)(2,1)S(1)} all-gather(bf16[224,512]{1,0:T(8,128)(2,1)S(1)} %multiply_convert_fusion), channel_id=1, replica_groups=mesh['grp'=2,'sp'=4,'tp'=4] {'tp'}, dimensions={1}, use_global_device_ids=true | all-gather | bytes 1146880 | tf_op jit(solution)/shard_map/all_gather | solution.py:56
  370.6 24.9 %all_to_all.100 = bf16[224,4,512]{2,0,1:T(8,128)(2,1)S(1)} all-to-all(bf16[224,4,512]{2,0,1:T(8,128)(2,1)S(1)} %bitcast.122), channel_id=1, replica_groups=mesh['grp'=2,'sp'=4,'tp'=4] {'sp'}, dimensions={1} | all-to-all | bytes 1835008 | tf_op jit(solution)/shard_map/all_to_all | solution.py:20
  395.5 1.1 convolution_convert_fusion
  396.6 44.7 %all_to_all.101 = bf16[4,224,1024]{2,1,0:T(8,128)(2,1)S(1)} all-to-all(bf16[4,224,1024]{2,1,0:T(8,128)(2,1)S(1)} %bitcast.129), channel_id=1, replica_groups=mesh['grp'=2,'sp'=4,'tp'=4] {'sp'}, dimensions={0} | all-to-all | bytes 3670016 | tf_op jit(solution)/shard_map/all_to_all | solution.py:27
  441.3 0.3 convert_reduce_fusion
  441.7 0.7 copy-done.2
  442.3 0.9 add_convert_fusion
  (38 shorter events, 0.5 us)
Async XLA Ops:
  6.5 24.0 %all-gather.3.cloned.1.call-start = ((), (), s32[]{:S(2)}) async-start(), calls=%async_computation.8 | async-start | bytes 2293760 | tf_op jit(solution)/shard_map/all_gather | solution.py:39
  30.5 2.1 copy-start
  34.5 4.7 %copy-start.3 = (bf16[2,1024,512]{2,1,0:T(8,128)(2,1)S(1)}, bf16[2,1024,512]{2,1,0:T(8,128)(2,1)}, u32[]{:S(2)}) copy-start(bf16[2,1024,512]{2,1,0:T(8,128)(2,1)} %param.11) | copy-start | bytes 6291460
  34.5 43.8 %all-to-all-start = ((bf16[224,4,1024]{2,0,1:T(8,128)(2,1)}), bf16[224,4,1024]{2,0,1:T(8,128)(2,1)}, u32[]{:S(2)}, u32[]{:S(2)}) async-start(bf16[224,4,1024]{2,0,1:T(8,128)(2,1)} %bitcast.115), calls=%async_computation | async-start | bytes 3670016 | tf_op jit(solution)/shard_map/all_to_all | solution.py:20
  83.8 6.8 %copy-start.7 = (f32[2,512]{1,0:T(2,128)S(1)}, f32[2,512]{1,0:T(2,128)}, u32[]{:S(2)}) copy-start(f32[2,512]{1,0:T(2,128)} %param.14) | copy-start | bytes 12292
  83.8 6.8 %copy-start.6 = (f32[2,31,512]{2,0,1:T(2,128)S(1)}, f32[2,31,512]{2,0,1:T(2,128)}, u32[]{:S(2)}) copy-start(f32[2,31,512]{2,0,1:T(2,128)} %param.12) | copy-start | bytes 380932
  83.8 45.9 %all-to-all-start.1 = ((bf16[4,224,1024]{2,1,0:T(8,128)(2,1)}), bf16[4,224,1024]{2,1,0:T(8,128)(2,1)S(1)}, u32[]{:S(2)}, u32[]{:S(2)}) async-start(bf16[4,224,1024]{2,1,0:T(8,128)(2,1)} %bitcast.125), calls=%async_computation.1 | async-start | bytes 3670016 | tf_op jit(solution)/shard_map/all_to_all | solution.py:27
  90.5 42.8 %copy-start.8 = (f32[2,512]{1,0:T(2,128)S(1)}, f32[2,512]{1,0:T(2,128)}, u32[]{:S(2)}) copy-start(f32[2,512]{1,0:T(2,128)} %param.13) | copy-start | bytes 12292
  90.5 160.7 %all-gather.5.cloned.1.call-start = ((), (), s32[]{:S(2)}) async-start(), calls=%async_computation.9 | async-start | bytes 2293760 | tf_op jit(solution)/shard_map/all_gather | solution.py:39
  130.2 4.7 %collective-permute-start = (bf16[30,512]{1,0:T(8,128)(2,1)S(1)}, bf16[30,512]{1,0:T(8,128)(2,1)S(1)}, u32[]{:S(2)}, u32[]{:S(2)}) collective-permute-start(bf16[30,512]{1,0:T(8,128)(2,1)S(1)} %slice.570), channel_id=1, source_target_pairs={{0,4},{4,8},{8,12},{1,5},{5,9},{9,13},{2,6},{6,10},{10,14},{3,7},{... | collective-permute-start | bytes 92168 | tf_op jit(solution)/shard_map/ppermute | solution.py:10
  155.2 25.5 %copy-start.9 = (bf16[2,512,1024]{2,1,0:T(8,128)(2,1)S(1)}, bf16[2,512,1024]{2,1,0:T(8,128)(2,1)}, u32[]{:S(2)}) copy-start(bf16[2,512,1024]{2,1,0:T(8,128)(2,1)} %param.15) | copy-start | bytes 6291460
  226.5 1.0 copy-start.4
  251.2 2.1 copy-start.1
  254.1 44.2 %copy-start.5 = (bf16[1024,512]{1,0:T(8,128)(2,1)S(1)}, bf16[1024,512]{1,0:T(8,128)(2,1)}, u32[]{:S(2)}) copy-start(bf16[1024,512]{1,0:T(8,128)(2,1)} %get-tuple-element.92) | copy-start | bytes 3145732
  345.5 4.8 %collective-permute-start.1 = (bf16[30,512]{1,0:T(8,128)(2,1)S(1)}, bf16[30,512]{1,0:T(8,128)(2,1)S(1)}, u32[]{:S(2)}, u32[]{:S(2)}) collective-permute-start(bf16[30,512]{1,0:T(8,128)(2,1)S(1)} %slice.604), channel_id=1, source_target_pairs={{0,4},{4,8},{8,12},{1,5},{5,9},{9,13},{2,6},{6,10},{10,14},{3,7},{... | collective-permute-start | bytes 92168 | tf_op jit(solution)/shard_map/ppermute | solution.py:10
  370.6 25.0 %copy-start.10 = (bf16[2,512,1024]{2,1,0:T(8,128)(2,1)S(1)}, bf16[2,512,1024]{2,1,0:T(8,128)(2,1)}, u32[]{:S(2)}) copy-start(bf16[2,512,1024]{2,1,0:T(8,128)(2,1)} %param.15) | copy-start | bytes 6291460
  441.3 1.0 copy-start.2
Sparse Core Ops, SparseCore 0:
  8.9 21.5 all-gather.2
  228.5 22.6 all-gather.4

commit v2 on v1

--- a/solution.py
+++ b/solution.py
@@ -1,7 +1,14 @@
+import functools
+
 import jax
 import jax.numpy as jnp
 from jax import lax
+from jax.experimental import pallas as pl
+from jax.experimental.pallas import tpu as pltpu
 from jax.sharding import PartitionSpec as P
+
+LANES = 128
+BF16, F32 = jnp.bfloat16, jnp.float32
 
 
 def passed_along(block, axis, distance):
@@ -28,7 +35,414 @@
     return jnp.sum(parts.astype(jnp.float32), axis=0)
 
 
+def send(src, dst, send_sem, recv_sem, **where):
+    return pltpu.make_async_remote_copy(
+        src_ref=src,
+        dst_ref=dst,
+        send_sem=send_sem,
+        recv_sem=recv_sem,
+        device_id=where,
+        device_id_type=pl.DeviceIdType.MESH,
+    )
+
+
+def gated_conv(
+    layer, sp, tp,
+    h_ref, gain_ref, wv_hbm, wg_hbm, taps_ref, lng_ref, lnb_ref, out_ref,
+    wv, wg, pieces, spread, xs, going, coming, own, sq, stat, halo_out, halo_in, ext, conv, acts,
+    w_sem, a_send, a_recv, b_send, c_send, c_relay, x_recv, r_send, r_recv,
+    q_send, q_recv, s_send, s_recv, h_send, h_recv, g_send, g_relay, g_recv,
+):
+    s, c = lax.axis_index("sp"), lax.axis_index("tp")
+    rows, depth = h_ref.shape
+    chans = taps_ref.shape[2]
+    part = depth // tp
+    step = going.shape[-1]
+    chunks = chans // step
+    pairs = tp // 2
+    sibling = c + 1 - 2 * (c % 2)
+    reach = taps_ref.shape[1]
+    pad = halo_in.shape[0]
+
+    loads = [
+        pltpu.make_async_copy(wv_hbm.at[layer], wv, w_sem.at[0]),
+        pltpu.make_async_copy(wg_hbm.at[layer], wg, w_sem.at[1]),
+    ]
+    for load in loads:
+        load.start()
+
+    barrier = pltpu.get_barrier_semaphore()
+    for j in range(1, tp):
+        pl.semaphore_signal(
+            barrier, inc=1, device_id={"tp": (c + j) % tp}, device_id_type=pl.DeviceIdType.MESH
+        )
+    for j in range(1, sp):
+        pl.semaphore_signal(
+            barrier, inc=1, device_id={"sp": (s + j) % sp}, device_id_type=pl.DeviceIdType.MESH
+        )
+
+    total = jnp.zeros((rows, LANES), F32)
+    for p in range(tp):
+        for lane in range(0, part, LANES):
+            at = p * part + lane
+            wide = h_ref[:, at : at + LANES].astype(F32)
+            total = total + wide * wide
+            pieces[p, :, lane : lane + LANES] = (
+                wide * gain_ref[0:1, at : at + LANES]
+            ).astype(BF16)
+    sq[c] = total
+    spread[c] = pieces[c]
+    pl.semaphore_wait(barrier, tp + sp - 2)
+
+    def a_copy(to, frm):
+        return send(pieces.at[to], spread.at[frm], a_send.at[to], a_recv.at[frm], tp=to)
+
+    def q_copy(to, frm):
+        return send(sq.at[frm], sq.at[frm], q_send.at[to], q_recv.at[frm], tp=to)
+
+    for j in range(1, tp):
+        a_copy((c + j) % tp, c).start()
+    for j in range(1, tp):
+        q_copy((c + j) % tp, c).start()
+
+    def b_copy(to, frm):
+        return send(spread.at[to], xs.at[c, frm], b_send.at[to], x_recv.at[c, frm], sp=to)
+
+    for j in range(1, sp + 1):
+        to = (s + j) % sp
+
+        @pl.when(to != c)
+        def _():
+            a_copy(c, to).wait_recv()
+
+        if j < sp:
+            b_copy(to, s).start()
+    xs[c, s] = spread[s]
+
+    def c_copy(to, d, sem):
+        return send(xs.at[c, d], xs.at[c, d], sem, x_recv.at[c, d], tp=to)
+
+    def relay(p, d):
+        return send(xs.at[p, d], xs.at[p, d], c_relay.at[p, d], x_recv.at[p, d], tp=sibling)
+
+    def arrived(p, d):
+        send(xs.at[p, d], xs.at[p, d], c_relay.at[p, d], x_recv.at[p, d], tp=sibling).wait_recv()
+
+    def gather(d):
+        @pl.when(d != s)
+        def _():
+            arrived(c, d)
+
+        for j in range(1, pairs):
+            c_copy((c + 2 * j) % tp, d, c_send.at[j, d]).start()
+        c_copy(sibling, d, c_send.at[0, d]).start()
+
+    def place(j):
+        left = j % 2
+        k = j // 2
+        d = (1 - left) * (sp - 1 - k) + left * k
+        return left, d, (1 - 2 * left) * (d - s) > 0
+
+    def each(body):
+        def one(j, carry):
+            left, d, valid = place(j)
+
+            @pl.when(valid)
+            def _():
+                body(left, d)
+
+            return carry
+
+        lax.fori_loop(0, 2 * (sp - 1), one, 0)
+
+    each(lambda left, d: gather(d))
+    gather(s)
+    for load in loads:
+        load.wait()
+
+    def ready(d):
+        for j in range(1, pairs):
+            p = (c + 2 * j) % tp
+            arrived(p, d)
+            relay(p, d).start()
+        for j in range(pairs):
+            arrived((sibling + 2 * j) % tp, d)
+
+    def product(d, weight, at):
+        acc = jnp.zeros((rows, step), F32)
+        for p in range(tp):
+            acc = acc + jnp.dot(
+                xs[p, d],
+                weight[p * part : (p + 1) * part, pl.ds(at, step)],
+                preferred_element_type=F32,
+            )
+        return acc
+
+    def r_copy(left, d, slot):
+        return send(
+            going.at[left, d, slot],
+            coming.at[left, d, slot],
+            r_send.at[left, d, slot],
+            r_recv.at[left, d, slot],
+            sp=s + 1 - 2 * left,
+        )
+
+    def r_arrived(left, d, slot):
+        send(
+            going.at[left, d, slot],
+            coming.at[left, d, slot],
+            r_send.at[left, d, slot],
+            r_recv.at[left, d, slot],
+            sp=(s + 1) % sp,
+        ).wait_recv()
+
+    def upstream(left):
+        return (1 - left) * s + left * (sp - 1 - s) > 0
+
+    def partial(left, d):
+        ready(d)
+        for half, weight in enumerate((wv, wg)):
+
+            def one(i, carry):
+                slot = half * chunks + i
+                own[half] = product(d, weight, pl.multiple_of(i * step, step))
+
+                @pl.when(upstream(left))
+                def _():
+                    r_arrived(left, d, slot)
+                    own[half] += coming[left, d, slot].astype(F32)
+
+                going[left, d, slot] = own[half].astype(BF16)
+                r_copy(left, d, slot).start()
+                return carry
+
+            lax.fori_loop(0, chunks, one, 0)
+
+    each(partial)
+
+    ready(s)
+    for j in range(1, tp):
+        q_copy(c, (c + j) % tp).wait_recv()
+    squares = sq[0]
+    for p in range(1, tp):
+        squares = squares + sq[p]
+    scale = lax.rsqrt(jnp.sum(squares, axis=1, keepdims=True) / (depth * tp) + 1e-06)
+
+    def finish(i, carry):
+        at = pl.multiple_of(i * step, step)
+        for half, weight in enumerate((wv, wg)):
+            slot = half * chunks + i
+            own[half] = product(s, weight, at)
+            for left in range(2):
+
+                @pl.when(upstream(left))
+                def _():
+                    r_arrived(left, s, slot)
+                    own[half] += coming[left, s, slot].astype(F32)
+
+        glu = (own[0] * scale * jax.nn.sigmoid(own[1] * scale)).astype(BF16)
+        ext[pad:, pl.ds(at, step)] = glu.astype(F32)
+        halo_out[:, pl.ds(at, step)] = glu[rows - pad :]
+        return carry
+
+    lax.fori_loop(0, chunks, finish, 0)
+
+    def h_copy(to):
+        return send(halo_out, halo_in, h_send, h_recv, sp=to)
+
+    @pl.when(s < sp - 1)
+    def _():
+        h_copy(s + 1).start()
+
+    @pl.when(s > 0)
+    def _():
+        h_copy((s + 1) % sp).wait_recv()
+        ext[:pad] = halo_in[...].astype(F32)
+
+    @pl.when(s == 0)
+    def _():
+        ext[:pad] = jnp.zeros((pad, chans), F32)
+
+    first = pad - (reach - 1)
+
+    def convolve(i, carry):
+        lanes = pl.ds(pl.multiple_of(i * LANES, LANES), LANES)
+        acc = jnp.zeros((rows, LANES), F32)
+        for k in range(reach):
+            acc = acc + taps_ref[0, k : k + 1, lanes] * ext[first + k : first + k + rows, lanes]
+        conv[:, lanes] = acc
+        return carry
+
+    lax.fori_loop(0, chans // LANES, convolve, 0)
+    whole = conv[...]
+    lane = lax.broadcasted_iota(jnp.int32, (rows, LANES), 1)
+    stat[c] = jnp.where(
+        lane == 0,
+        jnp.sum(whole, axis=1, keepdims=True),
+        jnp.sum(whole * whole, axis=1, keepdims=True),
+    )
+
+    def s_copy(to, frm):
+        return send(stat.at[frm], stat.at[frm], s_send.at[to], s_recv.at[frm], tp=to)
+
+    for j in range(1, tp):
+        s_copy((c + j) % tp, c).start()
+    for j in range(1, tp):
+        s_copy(c, (c + j) % tp).wait_recv()
+    stats = stat[0]
+    for p in range(1, tp):
+        stats = stats + stat[p]
+    mean = stats[:, 0:1] / (chans * tp)
+    var = stats[:, 1:2] / (chans * tp) - mean * mean
+    inv = lax.rsqrt(var + 1e-05)
+    for at in range(0, chans, LANES):
+        lanes = slice(at, at + LANES)
+        shaped = (conv[:, lanes] - mean) * inv * lng_ref[0:1, lanes] + lnb_ref[0:1, lanes]
+        acts[c, :, lanes] = (shaped / (1.0 + jnp.exp(-shaped))).astype(BF16)
+
+    def g_copy(to, p, sem):
+        return send(acts.at[p], acts.at[p], sem, g_recv.at[p], tp=to)
+
+    for j in range(1, pairs):
+        g_copy((c + 2 * j) % tp, c, g_send.at[j]).start()
+    g_copy(sibling, c, g_send.at[0]).start()
+    for j in range(1, pairs):
+        p = (c + 2 * j) % tp
+        g_copy(sibling, p, g_relay.at[p]).wait_recv()
+        g_copy(sibling, p, g_relay.at[p]).start()
+    for j in range(pairs):
+        p = (sibling + 2 * j) % tp
+        g_copy(sibling, p, g_relay.at[p]).wait_recv()
+    cut = out_ref.shape[3]
+    for p in range(tp):
+        for n in range(chans // cut):
+            out_ref[n, p] = acts[p, :, n * cut : (n + 1) * cut]
+
+    for j in range(1, tp):
+        a_copy((c + j) % tp, c).wait_send()
+        q_copy((c + j) % tp, c).wait_send()
+        s_copy((c + j) % tp, c).wait_send()
+    for j in range(1, sp):
+        b_copy((s + j) % sp, s).wait_send()
+
+    def sent(d, carry):
+        c_copy(sibling, d, c_send.at[0, d]).wait_send()
+        for j in range(1, pairs):
+            p = (c + 2 * j) % tp
+            c_copy(p, d, c_send.at[j, d]).wait_send()
+            relay(p, d).wait_send()
+        return carry
+
+    lax.fori_loop(0, sp, sent, 0)
+
+    def partial_sent(left, d):
+        def one(slot, carry):
+            r_copy(left, d, slot).wait_send()
+            return carry
+
+        lax.fori_loop(0, 2 * chunks, one, 0)
+
+    each(partial_sent)
+
+    @pl.when(s < sp - 1)
+    def _():
+        h_copy(s + 1).wait_send()
+
+    g_copy(sibling, c, g_send.at[0]).wait_send()
+    for j in range(1, pairs):
+        p = (c + 2 * j) % tp
+        g_copy(p, c, g_send.at[j]).wait_send()
+        g_copy(sibling, p, g_relay.at[p]).wait_send()
+
+
+def fused_branch(layer, cuts, h, gain, w_value, w_gate, taps, ln_gain, ln_bias):
+    sp, tp = lax.axis_size("sp"), lax.axis_size("tp")
+    rows, depth = h.shape
+    chans, reach = w_value.shape[2], taps.shape[1]
+    part, step = depth // tp, min(2 * LANES, chans)
+    slots = 2 * (chans // step)
+    pad = -(-(reach - 1) // 16) * 16
+    vmem, dma = pltpu.VMEM, pltpu.SemaphoreType.DMA
+    here = pl.BlockSpec(memory_space=pltpu.VMEM)
+    there = pl.BlockSpec(memory_space=pl.ANY)
+    return pl.pallas_call(
+        functools.partial(gated_conv, layer, sp, tp),
+        out_shape=jax.ShapeDtypeStruct((cuts, tp, rows, chans // cuts), BF16),
+        in_specs=[here, here, there, there, here, here, here],
+        out_specs=here,
+        scratch_shapes=[
+            vmem((depth, chans), BF16),
+            vmem((depth, chans), BF16),
+            vmem((tp, rows, part), BF16),
+            vmem((tp, rows, part), BF16),
+            vmem((tp, sp, rows, part), BF16),
+            vmem((2, sp, slots, rows, step), BF16),
+            vmem((2, sp, slots, rows, step), BF16),
+            vmem((2, rows, step), F32),
+            vmem((tp, rows, LANES), F32),
+            vmem((tp, rows, LANES), F32),
+            vmem((pad, chans), BF16),
+            vmem((pad, chans), BF16),
+            vmem((pad + rows, chans), F32),
+            vmem((rows, chans), F32),
+            vmem((tp, rows, chans), BF16),
+            dma((2,)), dma((tp,)), dma((tp,)), dma((sp,)), dma((tp, sp)), dma((tp, sp)),
+            dma((tp, sp)), dma((2, sp, slots)), dma((2, sp, slots)),
+            dma((tp,)), dma((tp,)), dma((tp,)), dma((tp,)), dma, dma,
+            dma((tp,)), dma((tp,)), dma((tp,)),
+        ],
+        compiler_params=pltpu.CompilerParams(
+            collective_id=layer, has_side_effects=True, vmem_limit_bytes=48 * 2**20
+        ),
+        cost_estimate=pl.CostEstimate(
+            flops=120_000_000_000, bytes_accessed=200_000_000, transcendentals=0
+        ),
+    )(h, gain, w_value, w_gate, taps, ln_gain, ln_bias)
+
+
+def gathered(weight):
+    grp = lax.axis_size("grp")
+    share = weight.shape[0] // grp
+    mine = lax.dynamic_slice_in_dim(weight, lax.axis_index("grp") * share, share, 0)
+    mine = lax.all_gather(mine, "sp", axis=0, tiled=True)
+    return lax.all_gather(mine, "grp", axis=0, tiled=True)
+
+
+def fits(tokens, w_value, taps):
+    sp, tp, grp = (lax.axis_size(a) for a in ("sp", "tp", "grp"))
+    rows, depth = tokens.shape
+    chans = w_value.shape[2]
+    return (
+        sp == tp
+        and tp % 2 == 0
+        and depth % (tp * LANES) == 0
+        and chans % (LANES * grp) == 0
+        and chans % min(2 * LANES, chans) == 0
+        and rows % 16 == 0
+        and rows >= -(-(taps.shape[1] - 1) // 16) * 16
+    )
+
+
+def fused(tokens, rms_gain, w_value, w_gate, taps, ln_gain, ln_bias, w_out):
+    grp = lax.axis_size("grp")
+    rows, depth = tokens.shape
+    gains = lax.dynamic_slice_in_dim(rms_gain, lax.axis_index("tp") * depth, depth, 1)
+    current = tokens
+    weights = [gathered(w_out[layer]) for layer in range(w_value.shape[0])]
+    for layer, weight in enumerate(weights):
+        one = slice(layer, layer + 1)
+        act = fused_branch(
+            layer, grp, current, gains[one], w_value, w_gate, taps[one], ln_gain[one], ln_bias[one]
+        )
+        act = act.transpose(2, 0, 1, 3).reshape(rows, -1)
+        branch = jnp.dot(act, weight, preferred_element_type=F32)
+        current = (current.astype(F32) + branch).astype(BF16)
+    return current
+
+
 def shards(tokens, rms_gain, w_value, w_gate, taps, ln_gain, ln_bias, w_out):
+    if fits(tokens, w_value, taps):
+        return fused(tokens, rms_gain, w_value, w_gate, taps, ln_gain, ln_bias, w_out)
     layers = w_value.shape[0]
     tok_rows = tokens.shape[0]
     chans = w_value.shape[2]

time: 456 us -> 289 us (0.63)
  blocking collectives: 264 us -> 0 us
  Pallas kernels: 0 us -> 181 us
  waiting for transfers between devices: 123 us -> 71.3 us
  starting transfers between devices: 18.6 us -> 0.12 us
  other arithmetic: 14 us -> 0 us
  local copies, waits for them, and re-layouts: 7.39 us -> 13.3 us
    all_to_all x6 -> x0, blocking collectives: 228 us -> none  [the longest x3 134 us: summed(): parts = lax.all_to_all(parts, 'sp', split_axis=0, concat_axis=0, tiled=True)]
    pallas_call x0 -> x2, Pallas kernels: none -> 181 us  [fused_branch(): pl.pallas_call(functools.partial(gated_conv, layer, sp, tp), out_shape=ja...]
    all_to_all x2 -> x0, waiting for transfers between devices: 74.9 us -> none  [the longest x1 39 us: summed(): parts = lax.all_to_all(parts, 'sp', split_axis=0, concat_axis=0, tiled=True)]
    all_gather x2 -> x4, waiting for transfers between devices: 45.2 us -> 71.2 us  [the longest x2 42.5 us: gathered(): mine = lax.all_gather(mine, 'sp', axis=0, tiled=True)]
    all_gather x2 -> x0, blocking collectives: 20.1 us -> none  [shards(): act_all = to_depth(lax.all_gather(act, 'tp', axis=1, tiled=True))]
    psum x2 -> x0, blocking collectives: 15.1 us -> none  [shards(): lax.psum((jnp.sum(conv, axis=1), jnp.sum(conv * conv, axis=1)), 'tp')]
    all_to_all x2 -> x0, starting transfers between devices: 11.5 us -> none  [the longest x1 6.78 us: summed(): parts = lax.all_to_all(parts, 'sp', split_axis=0, concat_axis=0, tiled=True)]
    reduce_sum x8 -> x0, other arithmetic: 10.2 us -> none  [the longest x2 4.77 us: shards(): jnp.sum(conv, axis=1)]
  transfers between devices with their start and end apart: 6 -> 4, of which waited for: 6 -> 2; matrix products, arithmetic and copies ran while one was open for 1% -> 4% of each run, Pallas kernels for 0% -> 63%
where the time goes in v2:
time: 289 us; the launch traced here: 287 us
  Pallas kernels  181 us (63%)
  waiting for transfers between devices  71.3 us (25%)
  local copies, waits for them, and re-layouts  13.3 us (5%)
  between operations  13.3 us (5%)
  matrix products  7.81 us (3%)
    pallas_call x2, Pallas kernels, fused_branch(): pl.pallas_call(functools.partial(gated_conv, layer, sp, tp), out_shape=ja...  181 us
    all_gather x2, waiting for transfers between devices, gathered(): mine = lax.all_gather(mine, 'sp', axis=0, tiled=True)  42.5 us
    all_gather x2, waiting for transfers between devices, gathered(): return lax.all_gather(mine, 'grp', axis=0, tiled=True)  28.7 us
    dot_general x2, matrix products, fused(): branch = jnp.dot(act, weight, preferred_element_type=F32)  7.81 us
  transfers between devices with their start and end apart: 4, of which 2 were waited for; matrix products, arithmetic and copies ran while one was open for 4% of the time, Pallas kernels for 63%

profile of v2, /device:TPU:21, one launch (start us, length us, event | category | flops | bytes accessed | tf_op | source)
XLA Modules:
  0.0 287.1 jit_solution(17757625864426494391)
XLA Ops:
  6.5 0.0 copy-start.4
  6.5 0.0 copy-start.5
  6.5 0.0 copy-start.6
  6.5 0.0 all-gather.9.cloned.1.call-start
  6.5 0.0 copy-start
  6.5 0.0 copy-start.3
  6.6 3.2 %fusion.16 = (bf16[1,512,1024]{2,1,0:T(8,128)(2,1)}, bf16[1,512,1024]{2,1,0:T(8,128)(2,1)}) fusion(bf16[2,512,1024]{2,1,0:T(8,128)(2,1)} %param.15), kind=kLoop, calls=%fused_computation.11 | loop fusion | bytes 4194304 | tf_op jit(solution)/shard_map/slice | solution.py:431
  9.8 1.9 constant_dynamic-slice_fusion.2
  11.6 0.0 all-gather.9.cloned.1.call-update
  11.6 0.0 all-gather.13.cloned.1.call-start
  11.7 1.9 constant_dynamic-slice_fusion.1
  13.6 0.0 all-gather.13.cloned.1.call-update
  13.6 0.0 all-gather.11.cloned.1.call-start
  13.7 0.0 copy-done.4
  13.7 0.1 fusion.17
  13.8 0.9 fusion.18
  14.7 0.0 copy-done.5
  14.7 0.0 copy-done.6
  14.7 42.5 %all-gather.9.cloned.1.call-done = bf16[1,1024,1024]{2,1,0:T(8,128)(2,1)} async-done(((bf16[1,256,1024]{2,1,0:T(8,128)(2,1)}), bf16[1,1024,1024]{2,1,0:T(8,128)(2,1)}) %all-gather.9.cloned.1.call-update) | async-done | bytes 2097168 | tf_op jit(solution)/shard_map/all_gather | solution.py:407
  57.1 0.0 all-gather.11.cloned.1.call-update
  57.2 0.0 all-gather.15.cloned.1.call-start
  57.2 0.0 copy-done
  57.2 0.0 copy-done.3
  57.2 0.0 copy-start.1
  57.2 1.6 copy-done.1
  58.8 101.8 %shard_map.82 = bf16[2,4,224,256]{3,2,1,0:T(8,128)(2,1)S(1)} custom-call(bf16[224,1024]{1,0:T(8,128)(2,1)S(1)} %copy-done.3, f32[1,1024]{1,0:T(1,128)S(1)} %get-tuple-element.10.gain_ref, bf16[2,1024,512]{2,1,0:T(8,128)(2,1)S(1)} %copy-done, bf16[2,1024,512]{2,1,0:T(8,128)(2,1)S(1)} %copy-done.1, f32[1,31,512]{2,1,0:T(8,128)S(1)} %copy.15.taps_ref, ...), custom_call_target="tpu_custom_call" | custom-call | flops 120000004096 | bytes 200000000 | tf_op jit(solution)/shard_map/pallas_call | solution.py:368
  160.7 0.7 copy.12
  161.4 1.7 reshape.8
  163.0 0.0 all-gather.13.cloned.1.call-done
  163.0 0.0 all-gather.15.cloned.1.call-update
  163.1 28.7 %all-gather.11.cloned.1.call-done = bf16[1,2048,1024]{2,1,0:T(8,128)(2,1)} async-done(((bf16[1,1024,1024]{2,1,0:T(8,128)(2,1)}), bf16[1,2048,1024]{2,1,0:T(8,128)(2,1)}) %all-gather.11.cloned.1.call-update) | async-done | bytes 4194320 | tf_op jit(solution)/shard_map/all_gather | solution.py:408
  191.8 0.0 copy-start.2
  191.8 3.7 %fusion.13.h_ref = bf16[224,1024]{1,0:T(8,128)(2,1)S(1)} fusion(bf16[224,2048]{1,0:T(8,128)(2,1)} %reshape.8, bf16[1,2048,1024]{2,1,0:T(8,128)(2,1)} %all-gather.11.cloned.1.call-done, bf16[224,1024]{1,0:T(8,128)(2,1)S(1)} %copy-done.3), kind=kOutput, calls=%fused_computation.7 | convolution fusion | flops 940212224 | bytes 6029312 | tf_op jit(solution)/shard_map/dot_general | solution.py:438
  195.5 0.0 copy-done.2
  195.5 79.5 %shard_map.83 = bf16[2,4,224,256]{3,2,1,0:T(8,128)(2,1)S(1)} custom-call(bf16[224,1024]{1,0:T(8,128)(2,1)S(1)} %fusion.13.h_ref, f32[1,1024]{1,0:T(1,128)S(1)} %get-tuple-element.9.gain_ref, bf16[2,1024,512]{2,1,0:T(8,128)(2,1)S(1)} %copy-done, bf16[2,1024,512]{2,1,0:T(8,128)(2,1)S(1)} %copy-done.2, f32[1,31,512]{2,1,0:T(8,128)S(1)} %copy.16.taps_ref, ...), custom_call_target="tpu_custom_call" | custom-call | flops 120000004096 | bytes 200000000 | tf_op jit(solution)/shard_map/pallas_call | solution.py:368
  275.0 0.7 copy.14
  275.7 0.7 reshape.9
  276.4 0.0 all-gather.15.cloned.1.call-done
  276.4 4.1 %fusion.10 = bf16[224,1024]{1,0:T(8,128)(2,1)} fusion(bf16[224,2048]{1,0:T(8,128)(2,1)S(1)} %reshape.9, bf16[1,2048,1024]{2,1,0:T(8,128)(2,1)} %all-gather.15.cloned.1.call-done, bf16[224,1024]{1,0:T(8,128)(2,1)S(1)} %fusion.13.h_ref), kind=kOutput, calls=%fused_computation.6 | convolution fusion | flops 940212224 | bytes 6029312 | tf_op jit(solution)/shard_map/dot_general | solution.py:438
  (3 shorter events, 0.0 us)
Async XLA Ops:
  6.5 7.1 %copy-start.4 = (f32[2,31,512]{2,0,1:T(2,128)S(1)}, f32[2,31,512]{2,0,1:T(2,128)}, u32[]{:S(2)}) copy-start(f32[2,31,512]{2,0,1:T(2,128)} %param.12) | copy-start | bytes 380932
  6.5 8.1 %copy-start.5 = (f32[2,512]{1,0:T(2,128)S(1)}, f32[2,512]{1,0:T(2,128)}, u32[]{:S(2)}) copy-start(f32[2,512]{1,0:T(2,128)} %param.14) | copy-start | bytes 12292
  6.5 8.1 %copy-start.6 = (f32[2,512]{1,0:T(2,128)S(1)}, f32[2,512]{1,0:T(2,128)}, u32[]{:S(2)}) copy-start(f32[2,512]{1,0:T(2,128)} %param.13) | copy-start | bytes 12292
  6.5 50.6 %all-gather.9.cloned.1.call-start = ((), (), s32[]{:S(2)}) async-start(), calls=%async_computation | async-start | bytes 2621440 | tf_op jit(solution)/shard_map/all_gather | solution.py:407
  6.5 50.7 %copy-start = (bf16[2,1024,512]{2,1,0:T(8,128)(2,1)S(1)}, bf16[2,1024,512]{2,1,0:T(8,128)(2,1)}, u32[]{:S(2)}) copy-start(bf16[2,1024,512]{2,1,0:T(8,128)(2,1)} %wv_hbm.3) | copy-start | bytes 6291460
  6.5 50.7 %copy-start.3 = (bf16[224,1024]{1,0:T(8,128)(2,1)S(1)}, bf16[224,1024]{1,0:T(8,128)(2,1)}, u32[]{:S(2)}) copy-start(bf16[224,1024]{1,0:T(8,128)(2,1)} %h_ref.1) | copy-start | bytes 1376260
  11.6 151.4 %all-gather.13.cloned.1.call-start = ((), (), s32[]{:S(2)}) async-start(), calls=%async_computation.2 | async-start | bytes 2621440 | tf_op jit(solution)/shard_map/all_gather | solution.py:407
  13.6 178.2 %all-gather.11.cloned.1.call-start = ((), (), s32[]{:S(2)}) async-start(), calls=%async_computation.1 | async-start | bytes 6291456 | tf_op jit(solution)/shard_map/all_gather | solution.py:408
  57.2 219.3 %all-gather.15.cloned.1.call-start = ((), (), s32[]{:S(2)}) async-start(), calls=%async_computation.3 | async-start | bytes 6291456 | tf_op jit(solution)/shard_map/all_gather | solution.py:408
  57.2 1.6 copy-start.1
  191.8 3.7 %copy-start.2 = (bf16[2,1024,512]{2,1,0:T(8,128)(2,1)S(1)}, bf16[2,1024,512]{2,1,0:T(8,128)(2,1)}, u32[]{:S(2)}) copy-start(bf16[2,1024,512]{2,1,0:T(8,128)(2,1)} %wg_hbm.3) | copy-start | bytes 6291460
Sparse Core Ops, SparseCore 0:
  11.8 45.3 all-gather.8
  58.7 74.7 all-gather.12
  135.0 56.7 all-gather.10
  193.2 56.7 all-gather.14

commit v3 on v2

--- a/solution.py
+++ b/solution.py
@@ -48,12 +48,15 @@
 
 def gated_conv(
     layer, sp, tp,
-    h_ref, gain_ref, wv_hbm, wg_hbm, taps_ref, lng_ref, lnb_ref, out_ref,
-    wv, wg, pieces, spread, xs, going, coming, own, sq, stat, halo_out, halo_in, ext, conv, acts,
+    h_ref, gain_ref, wv_hbm, wg_hbm, taps_ref, lng_ref, lnb_ref, wo_hbm, out_ref,
+    wv, wg, wo, pieces, spread, xs, going, coming, own, sq, stat, halo_out, halo_in, ext, conv, acts,
     w_sem, a_send, a_recv, b_send, c_send, c_relay, x_recv, r_send, r_recv,
     q_send, q_recv, s_send, s_recv, h_send, h_recv, g_send, g_relay, g_recv,
+    o_sem, z_send, z_recv, y_send, y_recv,
 ):
-    s, c = lax.axis_index("sp"), lax.axis_index("tp")
+    s, c, g = lax.axis_index("sp"), lax.axis_index("tp"), lax.axis_index("grp")
+    grp, share = wo.shape[1], wo.shape[2]
+    padded = sq.shape[2]
     rows, depth = h_ref.shape
     chans = taps_ref.shape[2]
     part = depth // tp
@@ -68,6 +71,12 @@
         pltpu.make_async_copy(wv_hbm.at[layer], wv, w_sem.at[0]),
         pltpu.make_async_copy(wg_hbm.at[layer], wg, w_sem.at[1]),
     ]
+    for n in range(grp):
+        loads.append(
+            pltpu.make_async_copy(
+                wo_hbm.at[layer, pl.ds(n * share, share)], wo.at[s, n], o_sem.at[n]
+            )
+        )
     for load in loads:
         load.start()
 
@@ -80,6 +89,17 @@
         pl.semaphore_signal(
             barrier, inc=1, device_id={"sp": (s + j) % sp}, device_id_type=pl.DeviceIdType.MESH
         )
+    for j in range(1, grp):
+        pl.semaphore_signal(
+            barrier, inc=1, device_id={"grp": (g + j) % grp}, device_id_type=pl.DeviceIdType.MESH
+        )
+
+    def to_row(column):
+        column = jnp.concatenate([column, jnp.zeros((padded - rows, LANES), F32)], axis=0)
+        return jnp.sum(column.T, axis=0, keepdims=True)
+
+    def to_column(row):
+        return jnp.broadcast_to(row, (LANES, padded)).T[:rows, 0:1]
 
     total = jnp.zeros((rows, LANES), F32)
     for p in range(tp):
@@ -90,9 +110,9 @@
             pieces[p, :, lane : lane + LANES] = (
                 wide * gain_ref[0:1, at : at + LANES]
             ).astype(BF16)
-    sq[c] = total
+    sq[c] = jnp.broadcast_to(to_row(total), sq.shape[1:])
     spread[c] = pieces[c]
-    pl.semaphore_wait(barrier, tp + sp - 2)
+    pl.semaphore_wait(barrier, tp + sp + grp - 3)
 
     def a_copy(to, frm):
         return send(pieces.at[to], spread.at[frm], a_send.at[to], a_recv.at[frm], tp=to)
@@ -104,6 +124,33 @@
         a_copy((c + j) % tp, c).start()
     for j in range(1, tp):
         q_copy((c + j) % tp, c).start()
+
+    def z_copy(left, o):
+        return send(
+            wo.at[o, g], wo.at[o, g], z_send.at[left, o], z_recv.at[o], sp=s + 1 - 2 * left
+        )
+
+    def y_copy(j, o, n):
+        return send(
+            wo.at[o, n], wo.at[o, n], y_send.at[j, o], y_recv.at[o, n], grp=(g + j) % grp
+        )
+
+    def pass_on(i):
+        for left in range(2):
+            o = s + (2 * left - 1) * i
+
+            @pl.when((o >= 0) & (o < sp))
+            def _():
+                send(
+                    wo.at[o, g], wo.at[o, g], z_send.at[left, o], z_recv.at[o], sp=(s + 1) % sp
+                ).wait_recv()
+
+                @pl.when((1 - left) * (sp - 1 - s) + left * s > 0)
+                def _():
+                    z_copy(left, o).start()
+
+                for j in range(1, grp):
+                    y_copy(j, o, g).start()
 
     def b_copy(to, frm):
         return send(spread.at[to], xs.at[c, frm], b_send.at[to], x_recv.at[c, frm], sp=to)
@@ -143,22 +190,31 @@
         d = (1 - left) * (sp - 1 - k) + left * k
         return left, d, (1 - 2 * left) * (d - s) > 0
 
-    def each(body):
+    def each(body, between=lambda j: None):
         def one(j, carry):
             left, d, valid = place(j)
+            between(j)
 
             @pl.when(valid)
             def _():
-                body(left, d)
+                body(j, left, d)
 
             return carry
 
         lax.fori_loop(0, 2 * (sp - 1), one, 0)
 
-    each(lambda left, d: gather(d))
+    each(lambda j, left, d: gather(d))
     gather(s)
     for load in loads:
         load.wait()
+
+    @pl.when(s < sp - 1)
+    def _():
+        z_copy(0, s).start()
+
+    @pl.when(s > 0)
+    def _():
+        z_copy(1, s).start()
 
     def ready(d):
         for j in range(1, pairs):
@@ -199,7 +255,7 @@
     def upstream(left):
         return (1 - left) * s + left * (sp - 1 - s) > 0
 
-    def partial(left, d):
+    def partial(j, left, d):
         ready(d)
         for half, weight in enumerate((wv, wg)):
 
@@ -218,15 +274,21 @@
 
             lax.fori_loop(0, chunks, one, 0)
 
-    each(partial)
-
+    def between(j):
+        for i in range(1, sp - 1):
+
+            @pl.when(j == 2 * i)
+            def _():
+                pass_on(i)
+
+    each(partial, between)
     ready(s)
     for j in range(1, tp):
         q_copy(c, (c + j) % tp).wait_recv()
     squares = sq[0]
     for p in range(1, tp):
         squares = squares + sq[p]
-    scale = lax.rsqrt(jnp.sum(squares, axis=1, keepdims=True) / (depth * tp) + 1e-06)
+    scale = to_column(lax.rsqrt(squares[0:1] / (depth * tp) + 1e-06))
 
     def finish(i, carry):
         at = pl.multiple_of(i * step, step)
@@ -263,6 +325,7 @@
     def _():
         ext[:pad] = jnp.zeros((pad, chans), F32)
 
+    pass_on(sp - 1)
     first = pad - (reach - 1)
 
     def convolve(i, carry):
@@ -274,12 +337,15 @@
         return carry
 
     lax.fori_loop(0, chans // LANES, convolve, 0)
-    whole = conv[...]
-    lane = lax.broadcasted_iota(jnp.int32, (rows, LANES), 1)
-    stat[c] = jnp.where(
-        lane == 0,
-        jnp.sum(whole, axis=1, keepdims=True),
-        jnp.sum(whole * whole, axis=1, keepdims=True),
+    total = jnp.zeros((rows, LANES), F32)
+    total_sq = jnp.zeros((rows, LANES), F32)
+    for at in range(0, chans, LANES):
+        tile = conv[:, at : at + LANES]
+        total = total + tile
+        total_sq = total_sq + tile * tile
+    half = sq.shape[1] // 2
+    stat[c] = jnp.concatenate(
+        [jnp.broadcast_to(to_row(t), (half, padded)) for t in (total, total_sq)], axis=0
     )
 
     def s_copy(to, frm):
@@ -292,9 +358,10 @@
     stats = stat[0]
     for p in range(1, tp):
         stats = stats + stat[p]
-    mean = stats[:, 0:1] / (chans * tp)
-    var = stats[:, 1:2] / (chans * tp) - mean * mean
-    inv = lax.rsqrt(var + 1e-05)
+    mean = stats[0:1] / (chans * tp)
+    var = stats[half : half + 1] / (chans * tp) - mean * mean
+    inv = to_column(lax.rsqrt(var + 1e-05))
+    mean = to_column(mean)
     for at in range(0, chans, LANES):
         lanes = slice(at, at + LANES)
         shaped = (conv[:, lanes] - mean) * inv * lng_ref[0:1, lanes] + lnb_ref[0:1, lanes]
@@ -313,10 +380,29 @@
     for j in range(pairs):
         p = (sibling + 2 * j) % tp
         g_copy(sibling, p, g_relay.at[p]).wait_recv()
-    cut = out_ref.shape[3]
-    for p in range(tp):
-        for n in range(chans // cut):
-            out_ref[n, p] = acts[p, :, n * cut : (n + 1) * cut]
+    for i in range(1, sp):
+        for left in range(2):
+            o = s + (2 * left - 1) * i
+
+            @pl.when((o >= 0) & (o < sp))
+            def _():
+                for j in range(1, grp):
+                    y_copy(j, o, (g + j) % grp).wait_recv()
+
+    def project(i, carry):
+        lanes = pl.ds(pl.multiple_of(i * step, step), step)
+        acc = jnp.zeros((rows, step), F32)
+        for p in range(tp):
+            for n in range(grp):
+                acc = acc + jnp.dot(
+                    acts[p, :, n * share : (n + 1) * share],
+                    wo[p, n, :, lanes],
+                    preferred_element_type=F32,
+                )
+        out_ref[:, lanes] = (h_ref[:, lanes].astype(F32) + acc).astype(BF16)
+        return carry
+
+    lax.fori_loop(0, depth // step, project, 0)
 
     for j in range(1, tp):
         a_copy((c + j) % tp, c).wait_send()
@@ -335,7 +421,7 @@
 
     lax.fori_loop(0, sp, sent, 0)
 
-    def partial_sent(left, d):
+    def partial_sent(j, left, d):
         def one(slot, carry):
             r_copy(left, d, slot).wait_send()
             return carry
@@ -347,6 +433,24 @@
     @pl.when(s < sp - 1)
     def _():
         h_copy(s + 1).wait_send()
+        z_copy(0, s).wait_send()
+
+    @pl.when(s > 0)
+    def _():
+        z_copy(1, s).wait_send()
+
+    for i in range(1, sp):
+        for left in range(2):
+            o = s + (2 * left - 1) * i
+
+            @pl.when((o >= 0) & (o < sp))
+            def _():
+                @pl.when((1 - left) * (sp - 1 - s) + left * s > 0)
+                def _():
+                    z_copy(left, o).wait_send()
+
+                for j in range(1, grp):
+                    y_copy(j, o, g).wait_send()
 
     g_copy(sibling, c, g_send.at[0]).wait_send()
     for j in range(1, pairs):
@@ -355,9 +459,10 @@
         g_copy(sibling, p, g_relay.at[p]).wait_send()
 
 
-def fused_branch(layer, cuts, h, gain, w_value, w_gate, taps, ln_gain, ln_bias):
-    sp, tp = lax.axis_size("sp"), lax.axis_size("tp")
+def fused_layer(layer, h, gain, w_value, w_gate, taps, ln_gain, ln_bias, w_out):
+    sp, tp, grp = (lax.axis_size(a) for a in ("sp", "tp", "grp"))
     rows, depth = h.shape
+    padded = -(-rows // LANES) * LANES
     chans, reach = w_value.shape[2], taps.shape[1]
     part, step = depth // tp, min(2 * LANES, chans)
     slots = 2 * (chans // step)
@@ -367,20 +472,21 @@
     there = pl.BlockSpec(memory_space=pl.ANY)
     return pl.pallas_call(
         functools.partial(gated_conv, layer, sp, tp),
-        out_shape=jax.ShapeDtypeStruct((cuts, tp, rows, chans // cuts), BF16),
-        in_specs=[here, here, there, there, here, here, here],
+        out_shape=jax.ShapeDtypeStruct((rows, depth), BF16),
+        in_specs=[here, here, there, there, here, here, here, there],
         out_specs=here,
         scratch_shapes=[
             vmem((depth, chans), BF16),
             vmem((depth, chans), BF16),
+            vmem((sp, grp, w_out.shape[1] // grp, depth), BF16),
             vmem((tp, rows, part), BF16),
             vmem((tp, rows, part), BF16),
             vmem((tp, sp, rows, part), BF16),
             vmem((2, sp, slots, rows, step), BF16),
             vmem((2, sp, slots, rows, step), BF16),
             vmem((2, rows, step), F32),
-            vmem((tp, rows, LANES), F32),
-            vmem((tp, rows, LANES), F32),
+            vmem((tp, 8, padded), F32),
+            vmem((tp, 8, padded), F32),
             vmem((pad, chans), BF16),
             vmem((pad, chans), BF16),
             vmem((pad + rows, chans), F32),
@@ -390,22 +496,12 @@
             dma((tp, sp)), dma((2, sp, slots)), dma((2, sp, slots)),
             dma((tp,)), dma((tp,)), dma((tp,)), dma((tp,)), dma, dma,
             dma((tp,)), dma((tp,)), dma((tp,)),
+            dma((grp,)), dma((2, sp)), dma((sp,)), dma((grp, sp)), dma((sp, grp)),
         ],
         compiler_params=pltpu.CompilerParams(
             collective_id=layer, has_side_effects=True, vmem_limit_bytes=48 * 2**20
         ),
-        cost_estimate=pl.CostEstimate(
-            flops=120_000_000_000, bytes_accessed=200_000_000, transcendentals=0
-        ),
-    )(h, gain, w_value, w_gate, taps, ln_gain, ln_bias)
-
-
-def gathered(weight):
-    grp = lax.axis_size("grp")
-    share = weight.shape[0] // grp
-    mine = lax.dynamic_slice_in_dim(weight, lax.axis_index("grp") * share, share, 0)
-    mine = lax.all_gather(mine, "sp", axis=0, tiled=True)
-    return lax.all_gather(mine, "grp", axis=0, tiled=True)
+    )(h, gain, w_value, w_gate, taps, ln_gain, ln_bias, w_out)
 
 
 def fits(tokens, w_value, taps):
@@ -424,19 +520,15 @@
 
 
 def fused(tokens, rms_gain, w_value, w_gate, taps, ln_gain, ln_bias, w_out):
-    grp = lax.axis_size("grp")
-    rows, depth = tokens.shape
+    depth = tokens.shape[1]
     gains = lax.dynamic_slice_in_dim(rms_gain, lax.axis_index("tp") * depth, depth, 1)
     current = tokens
-    weights = [gathered(w_out[layer]) for layer in range(w_value.shape[0])]
-    for layer, weight in enumerate(weights):
+    for layer in range(w_value.shape[0]):
         one = slice(layer, layer + 1)
-        act = fused_branch(
-            layer, grp, current, gains[one], w_value, w_gate, taps[one], ln_gain[one], ln_bias[one]
-        )
-        act = act.transpose(2, 0, 1, 3).reshape(rows, -1)
-        branch = jnp.dot(act, weight, preferred_element_type=F32)
-        current = (current.astype(F32) + branch).astype(BF16)
+        current = fused_layer(
+            layer, current, gains[one], w_value, w_gate, taps[one], ln_gain[one], ln_bias[one],
+            w_out,
+        )
     return current
 
 

time: 289 us -> 219 us (0.76)
  waiting for transfers between devices: 71.3 us -> 0 us
  Pallas kernels: 181 us -> 211 us
  between operations: 13.3 us -> 0.07 us
  matrix products: 7.81 us -> 0 us
  local copies, waits for them, and re-layouts: 13.3 us -> 7.7 us
    all_gather x4 -> x0, waiting for transfers between devices: 71.2 us -> none  [the longest x2 42.5 us: gathered(): mine = lax.all_gather(mine, 'sp', axis=0, tiled=True)]
    pallas_call x2, Pallas kernels: 181 us -> 211 us  [fused_layer(): pl.pallas_call(functools.partial(gated_conv, layer, sp, tp), out_shape=ja...]
    dot_general x2 -> x0, matrix products: 7.81 us -> none  [fused(): branch = jnp.dot(act, weight, preferred_element_type=F32)]
    dynamic_slice x2 -> x0, local copies, waits for them, and re-layouts: 3.75 us -> none  [gathered(): lax.dynamic_slice_in_dim(weight, lax.axis_index('grp') * share, share, 0)]
    unnamed x16 -> x13, local copies, waits for them, and re-layouts: 1.62 us -> 4.99 us
    slice x1 -> x0, local copies, waits for them, and re-layouts: 3.2 us -> none  [fused(): weights = [gathered(w_out[layer]) for layer in range(w_value.shape[0])]]
  transfers between devices with their start and end apart: 4 -> 0, of which waited for: 2 -> 0; matrix products, arithmetic and copies ran while one was open for 4% -> 0% of each run, Pallas kernels for 63% -> 0%
where the time goes in v3:
time: 219 us
  Pallas kernels  211 us (96%)
  local copies, waits for them, and re-layouts  7.7 us (4%)
    pallas_call x2, Pallas kernels, fused_layer(): pl.pallas_call(functools.partial(gated_conv, layer, sp, tp), out_shape=ja...  211 us
    unnamed x13, local copies, waits for them, and re-layouts  4.99 us

profile of v3, /device:TPU:21, one launch (start us, length us, event | category | flops | bytes accessed | tf_op | source)
XLA Modules:
  0.0 219.0 jit_solution(7608840763386073969)
XLA Ops:
  0.0 0.8 fusion.1
  0.8 0.8 fusion.2
  1.6 1.1 fusion
  2.8 0.0 copy-start
  2.8 1.6 copy-done
  4.3 0.0 copy-start.2
  4.3 1.6 copy-done.2
  5.9 0.0 copy-start.4
  5.9 1.0 copy-done.4
  7.0 0.0 copy-start.1
  7.0 0.0 copy-start.3
  7.0 106.5 %shard_map.82.h_ref = bf16[224,1024]{1,0:T(8,128)(2,1)S(1)} custom-call(bf16[224,1024]{1,0:T(8,128)(2,1)S(1)} %copy-done.4, f32[1,1024]{1,0:T(1,128)S(1)} %get-tuple-element.8.gain_ref, bf16[2,1024,512]{2,1,0:T(8,128)(2,1)S(1)} %copy-done, bf16[2,1024,512]{2,1,0:T(8,128)(2,1)S(1)} %copy-done.2, f32[1,31,512]{2,1,0:T(8,128)S(1)} %copy.11.taps_ref, ...), custom_call_target="tpu_custom_call" | custom-call | tf_op jit(solution)/shard_map/pallas_call | solution.py:473
  113.5 0.0 copy-done.1
  113.5 0.0 copy-done.3
  113.5 104.7 %shard_map.83 = bf16[224,1024]{1,0:T(8,128)(2,1)S(1)} custom-call(bf16[224,1024]{1,0:T(8,128)(2,1)S(1)} %shard_map.82.h_ref, f32[1,1024]{1,0:T(1,128)S(1)} %get-tuple-element.7.gain_ref, bf16[2,1024,512]{2,1,0:T(8,128)(2,1)S(1)} %copy-done.1, bf16[2,1024,512]{2,1,0:T(8,128)(2,1)S(1)} %copy-done.3, f32[1,31,512]{2,1,0:T(8,128)S(1)} %copy.12.taps_ref, ...), custom_call_target="tpu_custom_call" | custom-call | tf_op jit(solution)/shard_map/pallas_call | solution.py:473
  218.2 0.8 copy.14
  (2 shorter events, 0.0 us)
Async XLA Ops:
  2.8 1.6 copy-start
  4.3 1.6 copy-start.2
  5.9 1.0 copy-start.4
  7.0 106.6 %copy-start.1 = (bf16[2,1024,512]{2,1,0:T(8,128)(2,1)S(1)}, bf16[2,1024,512]{2,1,0:T(8,128)(2,1)}, u32[]{:S(2)}) copy-start(bf16[2,1024,512]{2,1,0:T(8,128)(2,1)} %wv_hbm.3) | copy-start | bytes 6291460
  7.0 106.6 %copy-start.3 = (bf16[2,1024,512]{2,1,0:T(8,128)(2,1)S(1)}, bf16[2,1024,512]{2,1,0:T(8,128)(2,1)}, u32[]{:S(2)}) copy-start(bf16[2,1024,512]{2,1,0:T(8,128)(2,1)} %wg_hbm.3) | copy-start | bytes 6291460

commit v4 on v3

--- a/solution.py
+++ b/solution.py
@@ -108,7 +108,7 @@
             wide = h_ref[:, at : at + LANES].astype(F32)
             total = total + wide * wide
             pieces[p, :, lane : lane + LANES] = (
-                wide * gain_ref[0:1, at : at + LANES]
+                wide * gain_ref[layer : layer + 1, pl.ds(pl.multiple_of(c * depth + at, LANES), LANES)]
             ).astype(BF16)
     sq[c] = jnp.broadcast_to(to_row(total), sq.shape[1:])
     spread[c] = pieces[c]
@@ -152,18 +152,50 @@
                 for j in range(1, grp):
                     y_copy(j, o, g).start()
 
+    for load in loads[2:]:
+        load.wait()
+
+    @pl.when(s < sp - 1)
+    def _():
+        z_copy(0, s).start()
+
+    @pl.when(s > 0)
+    def _():
+        z_copy(1, s).start()
+
     def b_copy(to, frm):
         return send(spread.at[to], xs.at[c, frm], b_send.at[to], x_recv.at[c, frm], sp=to)
 
-    for j in range(1, sp + 1):
-        to = (s + j) % sp
-
-        @pl.when(to != c)
+    def place(j):
+        left = (j + 2 * s // sp) % 2
+        k = j // 2
+        d = (1 - left) * (sp - 1 - k) + left * k
+        return left, d, (1 - 2 * left) * (d - s) > 0
+
+    def each(body, between=lambda j: None):
+        def one(j, carry):
+            left, d, valid = place(j)
+            between(j)
+
+            @pl.when(valid)
+            def _():
+                body(j, left, d)
+
+            return carry
+
+        lax.fori_loop(0, 2 * (sp - 1), one, 0)
+
+    def held(e):
+        @pl.when(e != c)
         def _():
-            a_copy(c, to).wait_recv()
-
-        if j < sp:
-            b_copy(to, s).start()
+            a_copy(c, e).wait_recv()
+
+    def scatter(j, left, d):
+        held(d)
+        b_copy(d, s).start()
+
+    each(scatter)
+    held(s)
     xs[c, s] = spread[s]
 
     def c_copy(to, d, sem):
@@ -184,37 +216,11 @@
             c_copy((c + 2 * j) % tp, d, c_send.at[j, d]).start()
         c_copy(sibling, d, c_send.at[0, d]).start()
 
-    def place(j):
-        left = j % 2
-        k = j // 2
-        d = (1 - left) * (sp - 1 - k) + left * k
-        return left, d, (1 - 2 * left) * (d - s) > 0
-
-    def each(body, between=lambda j: None):
-        def one(j, carry):
-            left, d, valid = place(j)
-            between(j)
-
-            @pl.when(valid)
-            def _():
-                body(j, left, d)
-
-            return carry
-
-        lax.fori_loop(0, 2 * (sp - 1), one, 0)
-
     each(lambda j, left, d: gather(d))
     gather(s)
-    for load in loads:
+    pass_on(1)
+    for load in loads[:2]:
         load.wait()
-
-    @pl.when(s < sp - 1)
-    def _():
-        z_copy(0, s).start()
-
-    @pl.when(s > 0)
-    def _():
-        z_copy(1, s).start()
 
     def ready(d):
         for j in range(1, pairs):
@@ -275,13 +281,14 @@
             lax.fori_loop(0, chunks, one, 0)
 
     def between(j):
-        for i in range(1, sp - 1):
+        for i in range(2, sp - 1):
 
             @pl.when(j == 2 * i)
             def _():
                 pass_on(i)
 
     each(partial, between)
+    pass_on(sp - 1)
     ready(s)
     for j in range(1, tp):
         q_copy(c, (c + j) % tp).wait_recv()
@@ -325,14 +332,13 @@
     def _():
         ext[:pad] = jnp.zeros((pad, chans), F32)
 
-    pass_on(sp - 1)
     first = pad - (reach - 1)
 
     def convolve(i, carry):
         lanes = pl.ds(pl.multiple_of(i * LANES, LANES), LANES)
         acc = jnp.zeros((rows, LANES), F32)
         for k in range(reach):
-            acc = acc + taps_ref[0, k : k + 1, lanes] * ext[first + k : first + k + rows, lanes]
+            acc = acc + taps_ref[layer, k : k + 1, lanes] * ext[first + k : first + k + rows, lanes]
         conv[:, lanes] = acc
         return carry
 
@@ -364,7 +370,7 @@
     mean = to_column(mean)
     for at in range(0, chans, LANES):
         lanes = slice(at, at + LANES)
-        shaped = (conv[:, lanes] - mean) * inv * lng_ref[0:1, lanes] + lnb_ref[0:1, lanes]
+        shaped = (conv[:, lanes] - mean) * inv * lng_ref[layer : layer + 1, lanes] + lnb_ref[layer : layer + 1, lanes]
         acts[c, :, lanes] = (shaped / (1.0 + jnp.exp(-shaped))).astype(BF16)
 
     def g_copy(to, p, sem):
@@ -520,14 +526,10 @@
 
 
 def fused(tokens, rms_gain, w_value, w_gate, taps, ln_gain, ln_bias, w_out):
-    depth = tokens.shape[1]
-    gains = lax.dynamic_slice_in_dim(rms_gain, lax.axis_index("tp") * depth, depth, 1)
     current = tokens
     for layer in range(w_value.shape[0]):
-        one = slice(layer, layer + 1)
         current = fused_layer(
-            layer, current, gains[one], w_value, w_gate, taps[one], ln_gain[one], ln_bias[one],
-            w_out,
+            layer, current, rms_gain, w_value, w_gate, taps, ln_gain, ln_bias, w_out
         )
     return current
 

time: 219 us -> 181 us (0.83)
  the two profiles are of different devices: /device:TPU:21 before, /device:TPU:15 now
where the time goes in v4:
time: 181 us; the launch traced here: 180 us
  Pallas kernels  172 us (95%)
  local copies, waits for them, and re-layouts  8.03 us (4%)
    pallas_call x2, Pallas kernels, fused_layer(): pl.pallas_call(functools.partial(gated_conv, layer, sp, tp), out_shape=ja...  172 us
    unnamed x18, local copies, waits for them, and re-layouts  8.03 us

profile of v4, /device:TPU:15, one launch (start us, length us, event | category | flops | bytes accessed | tf_op | source)
XLA Modules:
  0.0 180.4 jit_solution(863786590878342880)
XLA Ops:
  0.0 0.9 copy.9.taps_ref
  0.9 0.0 copy-start
  0.9 1.6 copy-done
  2.5 0.0 copy-start.2
  2.5 1.6 copy-done.2
  4.1 0.0 copy-start.4
  4.1 1.0 copy-done.4
  5.1 0.0 copy-start.5
  5.1 0.8 copy-done.5
  5.9 0.0 copy-start.6
  5.9 0.7 copy-done.6
  6.6 0.0 copy-start.7
  6.6 0.7 copy-done.7
  7.3 0.0 copy-start.1
  7.3 0.0 copy-start.3
  7.3 85.9 %shard_map.82.h_ref = bf16[224,1024]{1,0:T(8,128)(2,1)S(1)} custom-call(bf16[224,1024]{1,0:T(8,128)(2,1)S(1)} %copy-done.4, f32[2,4096]{1,0:T(2,128)S(1)} %copy-done.5, bf16[2,1024,512]{2,1,0:T(8,128)(2,1)S(1)} %copy-done, bf16[2,1024,512]{2,1,0:T(8,128)(2,1)S(1)} %copy-done.2, f32[2,31,512]{2,1,0:T(8,128)S(1)} %copy.9.taps_ref, f32[2,512]{1,0:T(2,128)S(1)} %copy-done.6, ...), custom_call_target="tpu_custom_call" | custom-call | tf_op jit(solution)/shard_map/pallas_call | solution.py:479
  93.2 0.0 copy-done.1
  93.2 0.0 copy-done.3
  93.2 86.4 %shard_map.83 = bf16[224,1024]{1,0:T(8,128)(2,1)S(1)} custom-call(bf16[224,1024]{1,0:T(8,128)(2,1)S(1)} %shard_map.82.h_ref, f32[2,4096]{1,0:T(2,128)S(1)} %copy-done.5, bf16[2,1024,512]{2,1,0:T(8,128)(2,1)S(1)} %copy-done.1, bf16[2,1024,512]{2,1,0:T(8,128)(2,1)S(1)} %copy-done.3, f32[2,31,512]{2,1,0:T(8,128)S(1)} %copy.9.taps_ref, f32[2,512]{1,0:T(2,128)S(1)} %copy-done.6, ...), custom_call_target="tpu_custom_call" | custom-call | tf_op jit(solution)/shard_map/pallas_call | solution.py:479
  179.6 0.8 copy.12
Async XLA Ops:
  0.9 1.6 copy-start
  2.5 1.6 copy-start.2
  4.1 1.0 copy-start.4
  5.1 0.8 copy-start.5
  5.9 0.7 copy-start.6
  6.6 0.7 copy-start.7
  7.3 85.9 %copy-start.1 = (bf16[2,1024,512]{2,1,0:T(8,128)(2,1)S(1)}, bf16[2,1024,512]{2,1,0:T(8,128)(2,1)}, u32[]{:S(2)}) copy-start(bf16[2,1024,512]{2,1,0:T(8,128)(2,1)} %wv_hbm.3) | copy-start | bytes 6291460
  7.3 85.9 %copy-start.3 = (bf16[2,1024,512]{2,1,0:T(8,128)(2,1)S(1)}, bf16[2,1024,512]{2,1,0:T(8,128)(2,1)}, u32[]{:S(2)}) copy-start(bf16[2,1024,512]{2,1,0:T(8,128)(2,1)} %wg_hbm.3) | copy-start | bytes 6291460
